TPU v7x, 32 devices: a whole 2x2x4 slice. The times are simulated.
32 devices in a mesh: grp: 2 (over y), fs: 4 (over z), tp: 4 (over x, core).
Axes of the slice: x: 2, y: 2, z: 4, core: 2. Of those that a mesh axis runs over, the one named last changes fastest.
Arguments:
- tokens: bfloat16 [4096, 2048], P(('grp', 'fs'), 'tp'), parts along dimension 0, may hold values from -16 to 16
- attn_gain: float32 [2048], replicated, may hold values from 0.1 to 1.9
- w_query: bfloat16 [2048, 1024], P('fs', 'tp'), may hold values from -0.125 to 0.125
- w_key: bfloat16 [2048, 1024], P('fs', 'tp'), may hold values from -0.125 to 0.125
- w_value: bfloat16 [2048, 2048], P('fs', 'tp'), may hold values from -0.125 to 0.125
- w_low: bfloat16 [2048, 32], replicated, may hold values from -0.125 to 0.125
- w_lift: bfloat16 [32, 1024], P(None, 'tp'), may hold values from -1 to 1
- decay_bias: float32 [1024], P('tp'), may hold values from -0.5 to 6
- head_gain: float32 [256], replicated, may hold values from 0.1 to 1.9
- w_out: bfloat16 [2048, 2048], P('tp', 'fs'), may hold values from -0.125 to 0.125
- ffn_gain: float32 [2048], replicated, may hold values from 0.1 to 1.9
- w_gate: bfloat16 [2048, 5632], P('fs', 'tp'), may hold values from -0.125 to 0.125
- w_up: bfloat16 [2048, 5632], P('fs', 'tp'), may hold values from -0.125 to 0.125
- w_down: bfloat16 [5632, 2048], P('tp', 'fs'), may hold values from -0.078125 to 0.078125
- final_gain: float32 [2048], P('tp'), may hold values from 0.1 to 1.9
Outputs:
- result: bfloat16 [4096, 2048], P(('grp', 'fs'), 'tp'), parts along dimension 0
There are 2 independent parts, one for each index of `grp`. A program takes and returns all parts, laid end to end along the dimension named above; an argument that names none is the same for every part. Nothing has to cross between parts.
All inputs are finite; a program needn't handle non-finite values.
Results may differ from a plain program's by a relative error of at most 0.015.
Values may be sent and summed in bfloat16 or wider, within the bound.
No kernel may reach another device: no remote copies, remote signals or barrier semaphores. Data moves between devices by JAX's collectives and lax.ppermute only.
A program may use at most 64 MiB of HBM per device.

v0:
```python
import jax
import jax.numpy as jnp
from jax import lax
from jax.sharding import PartitionSpec as P

D = 2048
DK = 128
DV = 256
BLOCK = 64


epsilon = 1e-06
highest = lax.Precision.HIGHEST


def rms_rows(values, gain):
    values = values.astype(jnp.float32)
    factor = lax.rsqrt(jnp.mean(values * values, axis=-1, keepdims=True) + epsilon)
    return values * factor * gain


def blockwise_gla(query_rows, key_rows, value_rows, log_decay, head_count):
    length = query_rows.shape[0]
    blocks = length // BLOCK

    def split_heads(array, depth):
        return (
            array.astype(jnp.float32)
            .reshape(blocks, BLOCK, head_count, depth)
            .transpose(2, 0, 1, 3)
        )

    query_f = split_heads(query_rows, DK) * DK ** (-0.5)
    key_f = split_heads(key_rows, DK)
    value_f = split_heads(value_rows, DV)
    log_cum = jnp.cumsum(split_heads(log_decay, DK), axis=2)
    log_last = log_cum[:, :, -1:, :]
    query_dec = query_f * jnp.exp(log_cum)
    key_dec = key_f * jnp.exp(-log_cum)
    causal = jnp.tril(jnp.ones((BLOCK, BLOCK), dtype=bool))
    scores = jnp.where(
        causal, jnp.einsum("hncd,hnsd->hncs", query_dec, key_dec, precision=highest), 0.0
    )
    inside = jnp.einsum("hncs,hnsv->hncv", scores, value_f, precision=highest)
    contrib = jnp.einsum(
        "hncd,hncv->hndv", key_f * jnp.exp(log_last - log_cum), value_f, precision=highest
    )
    decay_block = jnp.exp(log_last[:, :, 0, :])

    def advance(carry_state, inputs):
        decay_step, added = inputs
        return (decay_step[..., None] * carry_state + added, carry_state)

    start_state = jnp.zeros((head_count, DK, DV), jnp.float32)
    final_state, earlier = lax.scan(
        advance, start_state, (jnp.moveaxis(decay_block, 1, 0), jnp.moveaxis(contrib, 1, 0))
    )
    earlier = jnp.moveaxis(earlier, 0, 1)
    output = inside + jnp.einsum("hncd,hndv->hncv", query_dec, earlier, precision=highest)
    return output.transpose(1, 2, 0, 3).reshape(length, head_count, DV)


def body(
    tokens,
    attn_gain,
    w_query,
    w_key,
    w_value,
    w_low,
    w_lift,
    decay_bias,
    head_gain,
    w_out,
    ffn_gain,
    w_gate,
    w_up,
    w_down,
    final_gain,
):
    own_width = tokens.shape[1]
    row_count = tokens.shape[0]
    whole_rows = lax.all_gather(tokens, "tp", axis=1, tiled=True)
    normed = rms_rows(whole_rows, attn_gain).astype(jnp.bfloat16)

    def add_pieces(source, pieces):
        return tuple(
            (
                jnp.dot(source, weight_piece, preferred_element_type=jnp.float32)
                for weight_piece in pieces
            )
        )

    query_sum, key_sum, value_sum = add_pieces(
        normed,
        (
            lax.all_gather(w_query, "fs", axis=0, tiled=True),
            lax.all_gather(w_key, "fs", axis=0, tiled=True),
            lax.all_gather(w_value, "fs", axis=0, tiled=True),
        ),
    )
    query_rows = query_sum.astype(jnp.bfloat16)
    key_rows = key_sum.astype(jnp.bfloat16)
    value_rows = value_sum.astype(jnp.bfloat16)
    low_rank = jnp.dot(normed, w_low, preferred_element_type=jnp.float32).astype(jnp.bfloat16)
    log_decay = (
        jax.nn.log_sigmoid(
            jnp.dot(low_rank, w_lift, preferred_element_type=jnp.float32) + decay_bias
        )
        / 16.0
    )
    head_count = query_rows.shape[1] // DK
    gla_out = blockwise_gla(query_rows, key_rows, value_rows, log_decay, head_count)
    mixed_heads = (
        rms_rows(gla_out, head_gain).reshape(row_count, head_count * DV).astype(jnp.bfloat16)
    )
    out_terms = jnp.dot(
        mixed_heads,
        lax.all_gather(w_out, "fs", axis=1, tiled=True),
        preferred_element_type=jnp.float32,
    )
    total_sum = lax.psum(out_terms.astype(jnp.bfloat16), "tp").astype(jnp.float32)
    full_rows = (whole_rows.astype(jnp.float32) + total_sum).astype(jnp.bfloat16)
    first_sum = lax.dynamic_slice_in_dim(full_rows, lax.axis_index("tp") * own_width, own_width, 1)
    normed_ffn = rms_rows(full_rows, ffn_gain).astype(jnp.bfloat16)
    gate_rows, up_rows = add_pieces(
        normed_ffn,
        (
            lax.all_gather(w_gate, "fs", axis=0, tiled=True),
            lax.all_gather(w_up, "fs", axis=0, tiled=True),
        ),
    )
    hidden = (jax.nn.silu(gate_rows) * up_rows).astype(jnp.bfloat16)
    down_terms = jnp.dot(
        hidden, lax.all_gather(w_down, "fs", axis=1, tiled=True), preferred_element_type=jnp.float32
    )
    own_ffn = lax.psum_scatter(
        down_terms.astype(jnp.bfloat16), "tp", scatter_dimension=1, tiled=True
    ).astype(jnp.float32)
    second_sum = first_sum.astype(jnp.float32) + own_ffn
    square_sum = lax.psum(jnp.sum(second_sum * second_sum, axis=1), "tp")
    factor = lax.rsqrt(square_sum / D + epsilon)[:, None]
    return (second_sum * factor * final_gain).astype(jnp.bfloat16)


def solution(mesh):
    return jax.shard_map(
        body,
        mesh=mesh,
        in_specs=(
            P(("grp", "fs"), "tp"),
            P(),
            P("fs", "tp"),
            P("fs", "tp"),
            P("fs", "tp"),
            P(),
            P(None, "tp"),
            P("tp"),
            P(),
            P("tp", "fs"),
            P(),
            P("fs", "tp"),
            P("fs", "tp"),
            P("tp", "fs"),
            P("tp"),
        ),
        out_specs=P(("grp", "fs"), "tp"),
        check_vma=False,
    )
```

profile of v0, /device:TPU:0, one launch (start us, length us, event | category | flops | bytes accessed | tf_op | source)
XLA Modules:
  0.0 620.5 jit_solution(5567289836711899672)
XLA Ops:
  10.6 23.6 %all-gather.9.cloned.1.call-done = bf16[512,2048]{1,0:T(8,128)(2,1)} async-done(((bf16[512,512]{1,0:T(8,128)(2,1)}), bf16[512,2048]{1,0:T(8,128)(2,1)}) %all-gather.9.cloned.1.call-update) | async-done | bytes 2097168 | tf_op jit(solution)/shard_map/all_gather | solution.py:82
  34.2 2.2 fusion.3
  40.5 23.3 %all-gather.11.cloned.1.call-done = bf16[2048,256]{1,0:T(8,128)(2,1)} async-done(((bf16[512,256]{1,0:T(8,128)(2,1)}), bf16[2048,256]{1,0:T(8,128)(2,1)}) %all-gather.11.cloned.1.call-update) | async-done | bytes 1048592 | tf_op jit(solution)/shard_map/all_gather | solution.py:96
  63.8 2.0 fusion.13
  66.9 25.9 %all-gather.13.cloned.1.call-done = bf16[2048,256]{1,0:T(8,128)(2,1)} async-done(((bf16[512,256]{1,0:T(8,128)(2,1)}), bf16[2048,256]{1,0:T(8,128)(2,1)}) %all-gather.13.cloned.1.call-update) | async-done | bytes 1048592 | tf_op jit(solution)/shard_map/all_gather | solution.py:97
  95.8 43.4 %all-gather.15.cloned.1.call-done = bf16[2048,512]{1,0:T(8,128)(2,1)} async-done(((bf16[512,512]{1,0:T(8,128)(2,1)}), bf16[2048,512]{1,0:T(8,128)(2,1)}) %all-gather.15.cloned.1.call-update) | async-done | bytes 2097168 | tf_op jit(solution)/shard_map/all_gather | solution.py:98
  139.3 2.9 convolution_convert_fusion.2
  142.3 2.8 bitcast_multiply_fusion.1
  145.2 2.4 convolution_bitcast_fusion
  147.5 20.2 %while.13 = (s32[]{:T(128)}, f32[2,128,256]{2,1,0:T(8,128)S(1)}, f32[8,2,128,256]{3,2,1,0:T(8,128)}, f32[8,2,128]{2,0,1:T(8,128)}, f32[8,2,128,256]{3,2,1,0:T(8,128)}, /*index=5*/s32[]{:T(128)}, s32[]{:T(128)}) while((s32[]{:T(128)}, f32[2,128,256]{2,1,0:T(8,128)S(1)}, f32[8,2,128,256]{3,2,1,0:T(8,128)}, f32[8,2,128]{2,0,1:T(8,128)}, ...), condition=%wide.region_3.4_spmd.clone, body=%wide.region_2.3_spmd.clone.sunk | while | flops 262147 | bytes 1314400 | solution.py:55
  167.7 2.1 convolution_select_fusion
  169.8 2.9 fusion.8
  178.1 7.1 %all-gather.17.cloned.1.call-done = bf16[512,2048]{1,0:T(8,128)(2,1)} async-done(((bf16[512,512]{1,0:T(8,128)(2,1)}), bf16[512,2048]{1,0:T(8,128)(2,1)}) %all-gather.17.cloned.1.call-update) | async-done | bytes 2097168 | tf_op jit(solution)/shard_map/all_gather | solution.py:118
  185.2 4.5 convolution_convert_fusion
  192.3 47.8 %all-reduce.2.cloned.1.call-done = bf16[512,2048]{1,0:T(8,128)(2,1)} async-done(((bf16[512,2048]{1,0:T(8,128)(2,1)}), bf16[512,2048]{1,0:T(8,128)(2,1)}) %all-reduce.2.cloned.1.call-update) | async-done | bytes 2097168 | tf_op jit(solution)/shard_map/psum | solution.py:121
  240.1 3.9 fusion
  244.0 104.4 %all-gather.19.cloned.1.call-done = bf16[2048,1408]{1,0:T(8,128)(2,1)} async-done(((bf16[512,1408]{1,0:T(8,128)(2,1)}), bf16[2048,1408]{1,0:T(8,128)(2,1)}) %all-gather.19.cloned.1.call-update) | async-done | bytes 5767184 | tf_op jit(solution)/shard_map/all_gather | solution.py:128
  348.4 8.5 %fusion.17 = f32[512,1408]{1,0:T(8,128)} fusion(bf16[2048,1408]{1,0:T(8,128)(2,1)} %all-gather.19.cloned.1.call-done, bf16[512,2048]{1,0:T(8,128)(2,1)} %get-tuple-element.77, f32[2048]{0:T(1024)S(1)} %copy-done.14, f32[512]{0:T(512)S(1)} %add_rsqrt_fusion.2), kind=kOutput, calls=%fused_computation.40 | convolution fusion | flops 2956984320 | bytes 10758144 | tf_op jit(solution)/shard_map/dot_general | solution.py:88
  356.9 98.1 %all-gather.21.cloned.1.call-done = bf16[2048,1408]{1,0:T(8,128)(2,1)} async-done(((bf16[512,1408]{1,0:T(8,128)(2,1)}), bf16[2048,1408]{1,0:T(8,128)(2,1)}) %all-gather.21.cloned.1.call-update) | async-done | bytes 5767184 | tf_op jit(solution)/shard_map/all_gather | solution.py:129
  455.0 106.5 %all-gather.23.cloned.1.call-done = bf16[1408,2048]{1,0:T(8,128)(2,1)} async-done(((bf16[1408,512]{1,0:T(8,128)(2,1)}), bf16[1408,2048]{1,0:T(8,128)(2,1)}) %all-gather.23.cloned.1.call-update) | async-done | bytes 5767184 | tf_op jit(solution)/shard_map/all_gather | solution.py:134
  561.5 13.4 %convolution_convert_fusion.1 = bf16[512,2048]{1,0:T(8,128)(2,1)} fusion(bf16[1408,2048]{1,0:T(8,128)(2,1)} %all-gather.23.cloned.1.call-done, bf16[2048,1408]{1,0:T(8,128)(2,1)} %all-gather.21.cloned.1.call-done, f32[512,1408]{1,0:T(8,128)} %fusion.17, bf16[512,2048]{1,0:T(8,128)(2,1)S(1)} %copy-done.2, f32[2048]{0:T(1024)S(1)} %copy-done.14, ...), kind=kOutput, calls=%fused_computation.18 | convolution fusion | flops 5915148288 | bytes 18622464 | tf_op jit(solution)/shard_map/dot_general | solution.py:133
  575.0 29.6 %reduce-scatter.2.cloned.1.call-done = bf16[512,512]{1,0:T(8,128)(2,1)} async-done(((bf16[512,2048]{1,0:T(8,128)(2,1)}), bf16[512,512]{1,0:T(8,128)(2,1)}) %reduce-scatter.2.cloned.1.call-update) | async-done | bytes 524304 | tf_op jit(solution)/shard_map/reduce_scatter | solution.py:136
  605.8 5.8 psum.15
  611.6 2.0 multiply_convert_fusion
  (101 shorter events, 41.3 us)
Async XLA Ops:
  6.5 30.5 %copy-start = (bf16[2048,32]{0,1:T(8,128)(2,1)S(1)}, bf16[2048,32]{0,1:T(8,128)(2,1)}, u32[]{:S(2)}) copy-start(bf16[2048,32]{0,1:T(8,128)(2,1)} %param.22) | copy-start | bytes 393220
  6.5 3.5 copy-start.10
  6.5 30.5 %copy-start.11 = (bf16[32,256]{1,0:T(8,128)(2,1)S(1)}, bf16[32,256]{1,0:T(8,128)(2,1)}, u32[]{:S(2)}) copy-start(bf16[32,256]{1,0:T(8,128)(2,1)} %param.23) | copy-start | bytes 49156
  6.5 30.5 %copy-start.12 = (f32[2048]{0:T(1024)S(1)}, f32[2048]{0:T(1024)}, u32[]{:S(2)}) copy-start(f32[2048]{0:T(1024)} %param.18) | copy-start | bytes 24580
  6.5 30.5 %copy-start.15 = (f32[256]{0:T(256)S(1)}, f32[256]{0:T(256)}, u32[]{:S(2)}) copy-start(f32[256]{0:T(256)} %param.24) | copy-start | bytes 3076
  6.5 27.7 %all-gather.9.cloned.1.call-start = ((), (), s32[]{:S(2)}) async-start(), calls=%async_computation.1 | async-start | bytes 2621440 | tf_op jit(solution)/shard_map/all_gather | solution.py:82
  7.3 56.5 %all-gather.11.cloned.1.call-start = ((), (), s32[]{:S(2)}) async-start(), calls=%async_computation.2 | async-start | bytes 1310720 | tf_op jit(solution)/shard_map/all_gather | solution.py:96
  8.0 84.8 %all-gather.13.cloned.1.call-start = ((), (), s32[]{:S(2)}) async-start(), calls=%async_computation.3 | async-start | bytes 1310720 | tf_op jit(solution)/shard_map/all_gather | solution.py:97
  8.8 130.5 %all-gather.15.cloned.1.call-start = ((), (), s32[]{:S(2)}) async-start(), calls=%async_computation.4 | async-start | bytes 2621440 | tf_op jit(solution)/shard_map/all_gather | solution.py:98
  9.3 175.8 %all-gather.17.cloned.1.call-start = ((), (), s32[]{:S(2)}) async-start(), calls=%async_computation.5 | async-start | bytes 2621440 | tf_op jit(solution)/shard_map/all_gather | solution.py:118
  9.9 230.1 %all-reduce.2.cloned.1.call-start = ((), (), s32[]{:S(2)}) async-start(), calls=%async_computation.6 | async-start | bytes 4194304 | tf_op jit(solution)/shard_map/psum | solution.py:121
  34.2 2.8 copy-start.1
  40.5 52.3 %copy-start.9 = (f32[512]{0:T(512)S(1)}, f32[512]{0:T(512)}, u32[]{:S(2)}) copy-start(f32[512]{0:T(512)} %copy-done.8) | copy-start | bytes 6148
  40.5 52.3 %copy-start.13 = (f32[2048]{0:T(1024)S(1)}, f32[2048]{0:T(1024)}, u32[]{:S(2)}) copy-start(f32[2048]{0:T(1024)} %param.18) | copy-start | bytes 24580
  174.4 1.8 copy-start.3
  176.2 9.0 %copy-start.7 = (f32[1,2,2,128]{3,1,2,0:T(2,128)S(1)}, f32[1,2,2,128]{3,1,2,0:T(2,128)}, u32[]{:S(2)}) copy-start(f32[1,2,2,128]{3,1,2,0:T(2,128)} %copy.49) | copy-start | bytes 6148
  177.0 8.2 %copy-start.5 = (f32[64,8,2,256]{3,1,2,0:T(8,128)S(1)}, f32[64,8,2,256]{3,1,2,0:T(8,128)}, u32[]{:S(2)}) copy-start(f32[64,8,2,256]{3,1,2,0:T(8,128)} %copy.48) | copy-start | bytes 3145732
  189.7 158.7 %all-gather.19.cloned.1.call-start = ((), (), s32[]{:S(2)}) async-start(), calls=%async_computation.7 | async-start | bytes 7208960 | tf_op jit(solution)/shard_map/all_gather | solution.py:128
  190.5 264.5 %all-gather.21.cloned.1.call-start = ((), (), s32[]{:S(2)}) async-start(), calls=%async_computation.8 | async-start | bytes 7208960 | tf_op jit(solution)/shard_map/all_gather | solution.py:129
  191.2 370.3 %all-gather.23.cloned.1.call-start = ((), (), s32[]{:S(2)}) async-start(), calls=%async_computation.9 | async-start | bytes 7208960 | tf_op jit(solution)/shard_map/all_gather | solution.py:134
  192.0 156.5 %copy-start.14 = (f32[2048]{0:T(1024)S(1)}, f32[2048]{0:T(1024)}, u32[]{:S(2)}) copy-start(f32[2048]{0:T(1024)} %param.27) | copy-start | bytes 24580
  192.0 412.6 %reduce-scatter.2.cloned.1.call-start = ((), (), s32[]{:S(2)}) async-start(), calls=%async_computation.10 | async-start | bytes 2621440 | tf_op jit(solution)/shard_map/reduce_scatter | solution.py:136
  348.4 213.1 %copy-start.2 = (bf16[512,2048]{1,0:T(8,128)(2,1)S(1)}, bf16[512,2048]{1,0:T(8,128)(2,1)}, u32[]{:S(2)}) copy-start(bf16[512,2048]{1,0:T(8,128)(2,1)} %get-tuple-element.77) | copy-start | bytes 6291460
  574.9 36.7 %copy-start.6 = (f32[512]{0:T(512)S(1)}, f32[512]{0:T(512)}, u32[]{:S(2)}) copy-start(f32[512]{0:T(512)} %param.31) | copy-start | bytes 6148
  (2 other events, 1.3 us)
Sparse Core Ops, SparseCore 0:
  8.9 25.2 all-gather.8
  35.8 27.9 all-gather.10
  65.4 27.3 all-gather.12
  94.2 45.0 all-gather.14
  140.7 44.4 all-gather.16
  189.9 50.1 all-reduce.1
  241.6 106.7 all-gather.18
  350.0 104.9 all-gather.20
  456.6 104.9 all-gather.22
  575.1 29.4 reduce-scatter.1
where the time goes:
time: 622 us; the launch traced here: 621 us
  waiting for transfers between devices  515 us (83%)
  matrix products  43.5 us (7%)
  other arithmetic  27.3 us (4%)
  local copies, waits for them, and re-layouts  14.3 us (2%)
  between operations  13.7 us (2%)
    all_gather x1, waiting for transfers between devices, body(): lax.all_gather(w_down, 'fs', axis=1, tiled=True)  107 us
    all_gather x1, waiting for transfers between devices, body(): lax.all_gather(w_gate, 'fs', axis=0, tiled=True)  104 us
    all_gather x1, waiting for transfers between devices, body(): lax.all_gather(w_up, 'fs', axis=0, tiled=True)  98.1 us
    psum x1, waiting for transfers between devices, body(): lax.psum(out_terms.astype(jnp.bfloat16), 'tp').astype(jnp.float32)  47.8 us
    all_gather x1, waiting for transfers between devices, body(): lax.all_gather(w_value, 'fs', axis=0, tiled=True)  43.4 us
    reduce_scatter x1, waiting for transfers between devices, body(): lax.psum_scatter(down_terms.astype(jnp.bfloat16), 'tp', scatter_dimension...  29.6 us
    all_gather x1, waiting for transfers between devices, body(): lax.all_gather(w_key, 'fs', axis=0, tiled=True)  25.9 us
    all_gather x1, waiting for transfers between devices, body(): whole_rows = lax.all_gather(tokens, 'tp', axis=1, tiled=True)  23.6 us
  transfers between devices with their start and end apart: 10, of which 10 were waited for; matrix products, arithmetic and copies ran while one was open for 10% of the time, Pallas kernels for 0%

commit v1 on v0

v1 whole, which is shorter than its diff:
```python
import functools

import jax
import jax.numpy as jnp
from jax import lax
from jax.experimental import pallas as pl
from jax.experimental.pallas import tpu as pltpu
from jax.sharding import PartitionSpec as P

DK = 128
DV = 256
BLOCK = 64

epsilon = 1e-06
bf16 = jnp.bfloat16
f32 = jnp.float32


def mixer_kernel(heads, q_ref, k_ref, v_ref, low_ref, lift_ref, bias_ref, gain_ref, out_ref):
    length = q_ref.shape[0]
    row = lax.broadcasted_iota(jnp.int32, (BLOCK, BLOCK), 0)
    col = lax.broadcasted_iota(jnp.int32, (BLOCK, BLOCK), 1)
    causal = row >= col
    ones = causal.astype(f32)
    logits = jnp.dot(low_ref[...], lift_ref[...], preferred_element_type=f32) + bias_ref[...]
    decay = (jnp.minimum(logits, 0.0) - jnp.log1p(jnp.exp(-jnp.abs(logits)))) / 16.0
    states = [jnp.zeros((DK, DV), f32) for _ in range(heads)]
    for block in range(length // BLOCK):
        rows = slice(block * BLOCK, (block + 1) * BLOCK)
        cum = jnp.dot(
            ones, decay[rows], preferred_element_type=f32, precision=lax.Precision.HIGHEST
        )
        last = cum[BLOCK - 1 : BLOCK]
        grow = jnp.exp(cum)
        key = k_ref[rows, :].astype(f32)
        query_dec = (q_ref[rows, :].astype(f32) * (DK**-0.5) * grow).astype(bf16)
        key_dec = (key * jnp.exp(-cum)).astype(bf16)
        key_end = (key * jnp.exp(last - cum)).astype(bf16)
        step = jnp.exp(last)
        for head in range(heads):
            chan = slice(head * DK, (head + 1) * DK)
            vals = slice(head * DV, (head + 1) * DV)
            value = v_ref[rows, vals]
            scores = lax.dot_general(
                query_dec[:, chan],
                key_dec[:, chan],
                (((1,), (1,)), ((), ())),
                preferred_element_type=f32,
            )
            scores = jnp.where(causal, scores, 0.0).astype(bf16)
            out = jnp.dot(scores, value, preferred_element_type=f32)
            out += jnp.dot(
                query_dec[:, chan], states[head].astype(bf16), preferred_element_type=f32
            )
            added = lax.dot_general(
                key_end[:, chan], value, (((0,), (0,)), ((), ())), preferred_element_type=f32
            )
            states[head] = jnp.transpose(step[:, chan]) * states[head] + added
            factor = lax.rsqrt(jnp.mean(out * out, axis=-1, keepdims=True) + epsilon)
            out_ref[rows, vals] = (out * factor * gain_ref[...]).astype(bf16)


def mixer(query, key, value, low, lift, bias, gain):
    heads = query.shape[1] // DK
    spec = pl.BlockSpec(memory_space=pltpu.VMEM)
    return pl.pallas_call(
        functools.partial(mixer_kernel, heads),
        out_shape=jax.ShapeDtypeStruct(value.shape, bf16),
        in_specs=[spec] * 7,
        out_specs=spec,
        cost_estimate=pl.CostEstimate(
            flops=10_000_000_000, bytes_accessed=4_000_000, transcendentals=1_000_000
        ),
        name="mixer",
    )(query, key, value, low, lift, bias.reshape(1, -1), gain.reshape(1, -1))


def body(sizes, tokens, attn_gain, w_query, w_key, w_value, w_low, w_lift, decay_bias,
         head_gain, w_out, ffn_gain, w_gate, w_up, w_down, final_gain):
    n_grp, n_fs, n_tp = sizes
    rows, width = tokens.shape
    features = width * n_tp
    unit = features // (n_fs * n_grp)
    grp, fs, tp = (lax.axis_index(name) for name in ("grp", "fs", "tp"))

    def send(value, axis, pairs):
        return lax.ppermute(value, axis, pairs)

    def line(part):
        if n_fs == 4:
            near = send(part, "fs", [(0, 1), (1, 0), (2, 3), (3, 2)])
            first = send(part, "fs", [(1, 2), (2, 1)])
            second = send(near, "fs", [(1, 2), (2, 1)])
            first = first + send(first, "fs", [(1, 0), (2, 3)])
            second = second + send(second, "fs", [(1, 0), (2, 3)])
            return [near, first, second]
        right, left, rights, lefts = part, part, [], []
        for step in range(1, n_fs):
            right = send(right, "fs", [(i, i + 1) for i in range(step - 1, n_fs - 1)])
            left = send(left, "fs", [(i + 1, i) for i in range(n_fs - step)])
            rights.append(right)
            lefts.append(left)
        return [rights[s] + lefts[n_fs - 2 - s] for s in range(n_fs - 1)]

    if n_fs == 4:
        owners = [fs ^ 1, jnp.where(fs < 2, 2, 1), jnp.where(fs < 2, 3, 0)]
    else:
        owners = [(fs + n_fs - s) % n_fs for s in range(1, n_fs)]
    order = [fs * n_grp + i for i in range(n_grp)]
    for owner in owners:
        order += [owner * n_grp + (grp + k) % n_grp for k in range(n_grp)]

    def gather(shard, axis):
        size = shard.shape[axis] // n_grp
        part = lax.dynamic_slice_in_dim(shard, grp * size, size, axis)
        parts = [lax.slice_in_dim(shard, i * size, (i + 1) * size, axis=axis) for i in range(n_grp)]
        for got in line(part):
            parts.append(got)
            for k in range(1, n_grp):
                parts.append(send(got, "grp", [((i + k) % n_grp, i) for i in range(n_grp)]))
        return jnp.concatenate(parts, axis=axis)

    bits = [1 << i for i in range(n_tp.bit_length() - 1)]

    def flip(value, bit):
        return send(value, "tp", [(i, i ^ bit) for i in range(n_tp)])

    def gather_tp(own):
        held = own[None]
        for bit in reversed(bits):
            held = jnp.concatenate([held, flip(held, bit)], 0)
        index = [0]
        for bit in reversed(bits):
            index += [i ^ bit for i in index]
        return [held[index.index(r)] for r in range(n_tp)]

    def scatter_tp(blocks):
        owners_left = [0]
        have = {r: blocks(tp ^ r) for r in range(n_tp)}
        for bit in bits:
            keep = [r for r in have if not r & bit]
            sent = jnp.stack([have[r | bit] for r in keep])
            got = flip(sent, bit)
            have = {
                r: (have[r].astype(f32) + got[i].astype(f32)).astype(bf16 if bit != bits[-1] else f32)
                for i, r in enumerate(keep)
            }
        return have[0]

    per_tp = width // unit

    def norm_permuted(pieces, gain):
        squares = sum(
            jnp.sum(jnp.square(piece.astype(f32)), axis=1, keepdims=True) for piece in pieces
        )
        factor = lax.rsqrt(squares / features + epsilon)
        stack = jnp.stack(
            [piece[:, i * unit : (i + 1) * unit] for piece in pieces for i in range(per_tp)]
        )
        gains = gain.reshape(-1, 1, unit)
        parts = []
        for at in order:
            place = ((at // per_tp) ^ tp) * per_tp + at % per_tp
            part = lax.dynamic_index_in_dim(stack, place, 0, keepdims=False).astype(f32)
            scale = lax.dynamic_index_in_dim(gains, at, 0, keepdims=False)
            parts.append((part * factor * scale).astype(bf16))
        return jnp.concatenate(parts, axis=1)

    def dot(a, b):
        return jnp.dot(a, b, preferred_element_type=f32)

    def position(at):
        place = 0
        for i, value in enumerate(order):
            place = place + jnp.where(value == at, i, 0)
        return place

    places = [position(at) for at in range(n_fs * n_grp)]
    place_of = jnp.stack(places)

    def owner_blocks(terms):
        stack = jnp.stack([terms[:, i * unit : (i + 1) * unit] for i in range(len(order))])

        def block(owner):
            return jnp.concatenate(
                [
                    lax.dynamic_index_in_dim(stack, place_of[owner * per_tp + i], 0, keepdims=False)
                    for i in range(per_tp)
                ],
                axis=1,
            )

        return block

    mix_weights = gather(jnp.concatenate([w_query, w_key, w_value], axis=1), 0)
    out_weights = gather(w_out, 1)
    gate_weights = gather(w_gate, 0)
    up_weights = gather(w_up, 0)
    down_weights = gather(w_down, 1)

    normed = norm_permuted(gather_tp(tokens), attn_gain)
    mixed_in = dot(normed, mix_weights).astype(bf16)
    keys = w_query.shape[1]
    low_order = jnp.concatenate(
        [lax.dynamic_slice_in_dim(w_low, at * unit, unit, 0) for at in order], 0
    )
    low = dot(normed, low_order).astype(bf16)
    mixed = mixer(
        mixed_in[:, :keys], mixed_in[:, keys : 2 * keys], mixed_in[:, 2 * keys :],
        low, w_lift, decay_bias, head_gain,
    )
    out_terms = dot(mixed, out_weights).astype(bf16)
    attn = scatter_tp(owner_blocks(out_terms))
    first_sum = (tokens.astype(f32) + attn).astype(bf16)
    normed_ffn = norm_permuted(gather_tp(first_sum), ffn_gain)
    gate_rows = dot(normed_ffn, gate_weights)
    up_rows = dot(normed_ffn, up_weights)
    hidden = (jax.nn.silu(gate_rows) * up_rows).astype(bf16)
    down_terms = dot(hidden, down_weights).astype(bf16)
    second_sum = first_sum.astype(f32) + scatter_tp(owner_blocks(down_terms))
    squares = jnp.sum(second_sum * second_sum, axis=1)
    for bit in bits:
        squares = squares + flip(squares, bit)
    factor = lax.rsqrt(squares / features + epsilon)[:, None]
    return (second_sum * factor * final_gain).astype(bf16)


def solution(mesh):
    sizes = tuple(mesh.shape[name] for name in ("grp", "fs", "tp"))
    return jax.shard_map(
        functools.partial(body, sizes),
        mesh=mesh,
        in_specs=(
            P(("grp", "fs"), "tp"),
            P(),
            P("fs", "tp"),
            P("fs", "tp"),
            P("fs", "tp"),
            P(),
            P(None, "tp"),
            P("tp"),
            P(),
            P("tp", "fs"),
            P(),
            P("fs", "tp"),
            P("fs", "tp"),
            P("tp", "fs"),
            P("tp"),
        ),
        out_specs=P(("grp", "fs"), "tp"),
        check_vma=False,
    )
```

time: 622 us -> 359 us (0.58)
  waiting for transfers between devices: 515 us -> 189 us
  starting transfers between devices: 0.6 us -> 56.3 us
  local copies, waits for them, and re-layouts: 14.3 us -> 43.6 us
  matrix products: 43.5 us -> 25.1 us
    all_gather x8 -> x0, waiting for transfers between devices: 432 us -> none  [the longest x1 107 us: body(): lax.all_gather(w_down, 'fs', axis=1, tiled=True)]
    ppermute x0 -> x50, waiting for transfers between devices: none -> 189 us  [send(): return lax.ppermute(value, axis, pairs)]
    ppermute x0 -> x50, starting transfers between devices: none -> 56.3 us  [send(): return lax.ppermute(value, axis, pairs)]
    psum x1 -> x0, waiting for transfers between devices: 47.8 us -> none  [body(): lax.psum(out_terms.astype(jnp.bfloat16), 'tp').astype(jnp.float32)]
    reduce_scatter x1 -> x0, waiting for transfers between devices: 29.6 us -> none  [body(): lax.psum_scatter(down_terms.astype(jnp.bfloat16), 'tp', scatter_dimension...]
    unnamed x36 -> x97, local copies, waits for them, and re-layouts: 4.03 us -> 32.8 us
    dot_general x11 -> x5, matrix products: 43.5 us -> 25.1 us  [dot(): return jnp.dot(a, b, preferred_element_type=f32)]
    unnamed x1 -> x25, other arithmetic: 0.01 us -> 15.8 us
  transfers between devices with their start and end apart: 10 -> 50, of which waited for: 10 -> 19; matrix products, arithmetic and copies ran while one was open for 10% -> 18% of each run, Pallas kernels for 0% -> 2%
where the time goes in v1:
time: 359 us; the launch traced here: 358 us
  waiting for transfers between devices  189 us (53%)
  starting transfers between devices  56.3 us (16%)
  local copies, waits for them, and re-layouts  43.6 us (12%)
  matrix products  25.1 us (7%)
  other arithmetic  22 us (6%)
  between operations  16.4 us (5%)
  Pallas kernels  6.17 us (2%)
    ppermute x50, waiting for transfers between devices, send(): return lax.ppermute(value, axis, pairs)  189 us
    ppermute x50, starting transfers between devices, send(): return lax.ppermute(value, axis, pairs)  56.3 us
    unnamed x97, local copies, waits for them, and re-layouts  32.8 us
    dot_general x5, matrix products, dot(): return jnp.dot(a, b, preferred_element_type=f32)  25.1 us
    unnamed x25, other arithmetic  15.8 us
  transfers between devices with their start and end apart: 50, of which 19 were waited for; matrix products, arithmetic and copies ran while one was open for 18% of the time, Pallas kernels for 2%

profile of v1, /device:TPU:0, one launch (start us, length us, event | category | flops | bytes accessed | tf_op | source)
XLA Modules:
  0.0 358.2 jit_solution(18355935935914509581)
XLA Ops:
  2.1 3.1 collective-permute-start.2
  8.3 3.6 %collective-permute-start.10 = (bf16[512,256]{1,0:T(8,128)(2,1)}, bf16[512,256]{1,0:T(8,128)(2,1)}, u32[]{:S(2)}, u32[]{:S(2)}) collective-permute-start(bf16[512,256]{1,0:T(8,128)(2,1)} %constant_dynamic-slice_fusion.15), channel_id=1, source_target_pairs={{0,4},{4,0},{8,12},{12,8},{1,5},{5,1},{9,13},{13,9},{2,6},{6,2},{1... | collective-permute-start | bytes 786440 | tf_op jit(solution)/shard_map/ppermute | solution.py:87
  51.6 3.0 collective-permute-done.11
  59.6 16.1 %collective-permute-done.13 = bf16[512,256]{1,0:T(8,128)(2,1)S(1)} collective-permute-done((bf16[512,256]{1,0:T(8,128)(2,1)}, bf16[512,256]{1,0:T(8,128)(2,1)S(1)}, u32[]{:S(2)}, u32[]{:S(2)}) %collective-permute-start.13) | collective-permute-done | bytes 262176 | tf_op jit(solution)/shard_map/ppermute | solution.py:87
  79.9 3.9 %collective-permute-start.38 = (bf16[1408,256]{1,0:T(8,128)(2,1)S(1)}, bf16[1408,256]{1,0:T(8,128)(2,1)}, u32[]{:S(2)}, u32[]{:S(2)}) collective-permute-start(bf16[1408,256]{1,0:T(8,128)(2,1)S(1)} %copy-done.8), channel_id=1, source_target_pairs={{0,4},{4,0},{8,12},{12,8},{1,5},{5,1},{9,13},{13,9},{2,6},{6,2},{1... | collective-permute-start | bytes 2162696 | tf_op jit(solution)/shard_map/ppermute | solution.py:87
  87.9 21.7 %collective-permute-done.16 = bf16[512,256]{1,0:T(8,128)(2,1)S(1)} collective-permute-done((bf16[512,256]{1,0:T(8,128)(2,1)S(1)}, bf16[512,256]{1,0:T(8,128)(2,1)S(1)}, u32[]{:S(2)}, u32[]{:S(2)}) %collective-permute-start.16) | collective-permute-done | bytes 262176 | tf_op jit(solution)/shard_map/ppermute | solution.py:87
  117.9 3.0 collective-permute-done.17
  126.2 10.1 %collective-permute-done.23 = bf16[256,1408]{1,0:T(8,128)(2,1)S(1)} collective-permute-done((bf16[256,1408]{1,0:T(8,128)(2,1)S(1)}, bf16[256,1408]{1,0:T(8,128)(2,1)S(1)}, u32[]{:S(2)}, u32[]{:S(2)}) %collective-permute-start.23) | collective-permute-done | bytes 720928 | tf_op jit(solution)/shard_map/ppermute | solution.py:87
  137.2 11.6 %collective-permute-done.31 = bf16[256,1408]{1,0:T(8,128)(2,1)S(1)} collective-permute-done((bf16[256,1408]{1,0:T(8,128)(2,1)}, bf16[256,1408]{1,0:T(8,128)(2,1)S(1)}, u32[]{:S(2)}, u32[]{:S(2)}) %collective-permute-start.31) | collective-permute-done | bytes 720928 | tf_op jit(solution)/shard_map/ppermute | solution.py:87
  155.2 8.6 %collective-permute-done.39 = bf16[1408,256]{1,0:T(8,128)(2,1)S(1)} collective-permute-done((bf16[1408,256]{1,0:T(8,128)(2,1)}, bf16[1408,256]{1,0:T(8,128)(2,1)S(1)}, u32[]{:S(2)}, u32[]{:S(2)}) %collective-permute-start.39) | collective-permute-done | bytes 720928 | tf_op jit(solution)/shard_map/ppermute | solution.py:87
  166.1 8.0 %collective-permute-done.33 = bf16[256,1408]{1,0:T(8,128)(2,1)S(1)} collective-permute-done((bf16[256,1408]{1,0:T(8,128)(2,1)S(1)}, bf16[256,1408]{1,0:T(8,128)(2,1)S(1)}, u32[]{:S(2)}, u32[]{:S(2)}) %collective-permute-start.33) | collective-permute-done | bytes 720928 | tf_op jit(solution)/shard_map/ppermute | solution.py:87
  176.9 8.6 %collective-permute-done.41 = bf16[1408,256]{1,0:T(8,128)(2,1)S(1)} collective-permute-done((bf16[1408,256]{1,0:T(8,128)(2,1)S(1)}, bf16[1408,256]{1,0:T(8,128)(2,1)S(1)}, u32[]{:S(2)}, u32[]{:S(2)}) %collective-permute-start.41) | collective-permute-done | bytes 720928 | tf_op jit(solution)/shard_map/ppermute | solution.py:87
  190.4 9.9 %collective-permute-done.6 = bf16[256,1024]{1,0:T(8,128)(2,1)S(1)} collective-permute-done((bf16[256,1024]{1,0:T(8,128)(2,1)S(1)}, bf16[256,1024]{1,0:T(8,128)(2,1)S(1)}, u32[]{:S(2)}, u32[]{:S(2)}) %collective-permute-start.6) | collective-permute-done | bytes 524320 | tf_op jit(solution)/shard_map/ppermute | solution.py:87
  206.7 24.0 %collective-permute-done.9 = bf16[256,1024]{1,0:T(8,128)(2,1)S(1)} collective-permute-done((bf16[256,1024]{1,0:T(8,128)(2,1)S(1)}, bf16[256,1024]{1,0:T(8,128)(2,1)S(1)}, u32[]{:S(2)}, u32[]{:S(2)}) %collective-permute-start.9) | collective-permute-done | bytes 524320 | tf_op jit(solution)/shard_map/ppermute | solution.py:87
  236.3 6.2 %mixer.1 = bf16[512,512]{1,0:T(8,128)(2,1)} custom-call(bf16[512,256]{1,0:T(8,128)(2,1)} %get-tuple-element.50.q_ref, bf16[512,256]{1,0:T(8,128)(2,1)} %get-tuple-element.49.k_ref, bf16[512,512]{1,0:T(8,128)(2,1)} %slice.197.v_ref, bf16[512,32]{1,0:T(8,128)(2,1)} %convolution_convert_fusion.3.low_ref, bf16[32,256]{1,0:T(8,128)(2,1)} %lift_ref.1, ...), custom_call_target="tpu_custom_call" | custom-call | flops 10000000000 | bytes 4000000 | tf_op jit(solution)/shard_map/mixer/pallas_call | solution.py:66
  242.5 3.0 convolution_convert_fusion
  257.7 13.5 %collective-permute-done.36 = bf16[256,1408]{1,0:T(8,128)(2,1)S(1)} collective-permute-done((bf16[256,1408]{1,0:T(8,128)(2,1)}, bf16[256,1408]{1,0:T(8,128)(2,1)S(1)}, u32[]{:S(2)}, u32[]{:S(2)}) %collective-permute-start.36) | collective-permute-done | bytes 720928 | tf_op jit(solution)/shard_map/ppermute | solution.py:87
  277.0 7.1 %collective-permute-done.44 = bf16[1408,256]{1,0:T(8,128)(2,1)S(1)} collective-permute-done((bf16[1408,256]{1,0:T(8,128)(2,1)}, bf16[1408,256]{1,0:T(8,128)(2,1)S(1)}, u32[]{:S(2)}, u32[]{:S(2)}) %collective-permute-start.44) | collective-permute-done | bytes 720928 | tf_op jit(solution)/shard_map/ppermute | solution.py:87
  288.4 11.2 %collective-permute-done.37 = bf16[256,1408]{1,0:T(8,128)(2,1)S(1)} collective-permute-done((bf16[256,1408]{1,0:T(8,128)(2,1)S(1)}, bf16[256,1408]{1,0:T(8,128)(2,1)S(1)}, u32[]{:S(2)}, u32[]{:S(2)}) %collective-permute-start.37) | collective-permute-done | bytes 720928 | tf_op jit(solution)/shard_map/ppermute | solution.py:87
  300.6 12.0 %collective-permute-done.45 = bf16[1408,256]{1,0:T(8,128)(2,1)S(1)} collective-permute-done((bf16[1408,256]{1,0:T(8,128)(2,1)S(1)}, bf16[1408,256]{1,0:T(8,128)(2,1)S(1)}, u32[]{:S(2)}, u32[]{:S(2)}) %collective-permute-start.45) | collective-permute-done | bytes 720928 | tf_op jit(solution)/shard_map/ppermute | solution.py:87
  316.7 5.0 %fusion.92 = f32[512,1408]{1,0:T(8,128)} fusion(bf16[512,2048]{1,0:T(8,128)(2,1)S(1)} %fusion.55, bf16[2048,1408]{1,0:T(8,128)(2,1)S(1)} %constant_dynamic-update-slice_fusion.24), kind=kOutput, calls=%fused_computation.262 | convolution fusion | flops 2952790016 | bytes 10747904 | tf_op jit(solution)/shard_map/dot_general | solution.py:170
  321.7 12.5 %convolution_convert_fusion.1 = bf16[512,2048]{1,0:T(8,128)(2,1)S(1)} fusion(bf16[1408,2048]{1,0:T(8,128)(2,1)} %constant_dynamic-update-slice_fusion.38, f32[512,1408]{1,0:T(8,128)} %fusion.92, bf16[512,2048]{1,0:T(8,128)(2,1)} %copy-done.13, bf16[2048,1408]{1,0:T(8,128)(2,1)} %constant_dynamic-update-slice_fusion.31), kind=kOutput, calls=%fused_computation.1 | convolution fusion | flops 5910953984 | bytes 18612224 | tf_op jit(solution)/shard_map/dot_general | solution.py:170
  338.4 13.4 %collective-permute-done.47 = bf16[1,512,512]{2,1,0:T(8,128)(2,1)S(1)} collective-permute-done((bf16[1,512,512]{2,1,0:T(8,128)(2,1)S(1)}, bf16[1,512,512]{2,1,0:T(8,128)(2,1)S(1)}, u32[]{:S(2)}, u32[]{:S(2)}) %collective-permute-start.47) | collective-permute-done | bytes 524320 | tf_op jit(solution)/shard_map/ppermute | solution.py:87
  354.0 3.0 collective-permute-done.49
  (252 shorter events, 119.7 us)
Async XLA Ops:
  2.1 76.1 %collective-permute-start.2 = (bf16[256,1024]{1,0:T(8,128)(2,1)}, bf16[256,1024]{1,0:T(8,128)(2,1)}, u32[]{:S(2)}, u32[]{:S(2)}) collective-permute-start(bf16[256,1024]{1,0:T(8,128)(2,1)} %fusion.7), channel_id=1, source_target_pairs={{0,4},{4,0},{8,12},{12,8},{1,5},{5,1},{9,13},{13,9},{2,6},{6,2},{1... | collective-permute-start | bytes 1572872 | tf_op jit(solution)/shard_map/ppermute | solution.py:87
  5.2 82.3 %collective-permute-start.4 = (bf16[256,1024]{1,0:T(8,128)(2,1)}, bf16[256,1024]{1,0:T(8,128)(2,1)}, u32[]{:S(2)}, u32[]{:S(2)}) collective-permute-start(bf16[256,1024]{1,0:T(8,128)(2,1)} %fusion.7), channel_id=1, source_target_pairs={{4,8},{8,4},{5,9},{9,5},{6,10},{10,6},{7,11},{11,7},{20,24},{24,20... | collective-permute-start | bytes 1572872 | tf_op jit(solution)/shard_map/ppermute | solution.py:87
  8.3 39.2 %collective-permute-start.10 = (bf16[512,256]{1,0:T(8,128)(2,1)}, bf16[512,256]{1,0:T(8,128)(2,1)}, u32[]{:S(2)}, u32[]{:S(2)}) collective-permute-start(bf16[512,256]{1,0:T(8,128)(2,1)} %constant_dynamic-slice_fusion.15), channel_id=1, source_target_pairs={{0,4},{4,0},{8,12},{12,8},{1,5},{5,1},{9,13},{13,9},{2,6},{6,2},{1... | collective-permute-start | bytes 786440 | tf_op jit(solution)/shard_map/ppermute | solution.py:87
  11.9 39.0 %collective-permute-start.12 = (bf16[512,256]{1,0:T(8,128)(2,1)}, bf16[512,256]{1,0:T(8,128)(2,1)}, u32[]{:S(2)}, u32[]{:S(2)}) collective-permute-start(bf16[512,256]{1,0:T(8,128)(2,1)} %constant_dynamic-slice_fusion.15), channel_id=1, source_target_pairs={{4,8},{8,4},{5,9},{9,5},{6,10},{10,6},{7,11},{11,7},{20,24},{24,20... | collective-permute-start | bytes 786440 | tf_op jit(solution)/shard_map/ppermute | solution.py:87
  13.3 43.5 %collective-permute-start = (bf16[1,512,512]{2,1,0:T(8,128)(2,1)S(1)}, bf16[1,512,512]{2,1,0:T(8,128)(2,1)S(1)}, u32[]{:S(2)}, u32[]{:S(2)}) collective-permute-start(bf16[1,512,512]{2,1,0:T(8,128)(2,1)S(1)} %bitcast.298), channel_id=1, source_target_pairs={{0,2},{1,3},{2,0},{3,1},{4,6},{5,7},{6,4},{7,5},{8,10},{9,11},{10,... | collective-permute-start | bytes 1572872 | tf_op jit(solution)/shard_map/ppermute | solution.py:87
  50.9 32.8 %collective-permute-start.22 = (bf16[256,1408]{1,0:T(8,128)(2,1)S(1)}, bf16[256,1408]{1,0:T(8,128)(2,1)S(1)}, u32[]{:S(2)}, u32[]{:S(2)}) collective-permute-start(bf16[256,1408]{1,0:T(8,128)(2,1)S(1)} %copy-done.10), channel_id=1, source_target_pairs={{0,4},{4,0},{8,12},{12,8},{1,5},{5,1},{9,13},{13,9},{2,6},{6,2},{1... | collective-permute-start | bytes 2162696 | tf_op jit(solution)/shard_map/ppermute | solution.py:87
  56.7 55.0 %collective-permute-start.30 = (bf16[256,1408]{1,0:T(8,128)(2,1)S(1)}, bf16[256,1408]{1,0:T(8,128)(2,1)}, u32[]{:S(2)}, u32[]{:S(2)}) collective-permute-start(bf16[256,1408]{1,0:T(8,128)(2,1)S(1)} %copy-done.9), channel_id=1, source_target_pairs={{0,4},{4,0},{8,12},{12,8},{1,5},{5,1},{9,13},{13,9},{2,6},{6,2},{1... | collective-permute-start | bytes 2162696 | tf_op jit(solution)/shard_map/ppermute | solution.py:87
  79.9 34.4 %collective-permute-start.38 = (bf16[1408,256]{1,0:T(8,128)(2,1)S(1)}, bf16[1408,256]{1,0:T(8,128)(2,1)}, u32[]{:S(2)}, u32[]{:S(2)}) collective-permute-start(bf16[1408,256]{1,0:T(8,128)(2,1)S(1)} %copy-done.8), channel_id=1, source_target_pairs={{0,4},{4,0},{8,12},{12,8},{1,5},{5,1},{9,13},{13,9},{2,6},{6,2},{1... | collective-permute-start | bytes 2162696 | tf_op jit(solution)/shard_map/ppermute | solution.py:87
  86.0 36.9 %collective-permute-start.24 = (bf16[256,1408]{1,0:T(8,128)(2,1)S(1)}, bf16[256,1408]{1,0:T(8,128)(2,1)S(1)}, u32[]{:S(2)}, u32[]{:S(2)}) collective-permute-start(bf16[256,1408]{1,0:T(8,128)(2,1)S(1)} %copy-done.10), channel_id=1, source_target_pairs={{4,8},{8,4},{5,9},{9,5},{6,10},{10,6},{7,11},{11,7},{20,24},{24,20... | collective-permute-start | bytes 2162696 | tf_op jit(solution)/shard_map/ppermute | solution.py:87
  87.4 34.7 %collective-permute-start.3 = (bf16[256,1024]{1,0:T(8,128)(2,1)}, bf16[256,1024]{1,0:T(8,128)(2,1)S(1)}, u32[]{:S(2)}, u32[]{:S(2)}) collective-permute-start(bf16[256,1024]{1,0:T(8,128)(2,1)} %collective-permute-done.2), channel_id=1, source_target_pairs={{16,0},{0,16},{17,1},{1,17},{18,2},{2,18},{19,3},{3,19},{20,4},{4,... | collective-permute-start | bytes 1572872 | tf_op jit(solution)/shard_map/ppermute | solution.py:87
  120.9 28.0 %collective-permute-start.31 = (bf16[256,1408]{1,0:T(8,128)(2,1)}, bf16[256,1408]{1,0:T(8,128)(2,1)S(1)}, u32[]{:S(2)}, u32[]{:S(2)}) collective-permute-start(bf16[256,1408]{1,0:T(8,128)(2,1)} %collective-permute-done.30), channel_id=1, source_target_pairs={{16,0},{0,16},{17,1},{1,17},{18,2},{2,18},{19,3},{3,19},{20,4},{4,... | collective-permute-start | bytes 2162696 | tf_op jit(solution)/shard_map/ppermute | solution.py:87
  122.1 28.2 %collective-permute-start.32 = (bf16[256,1408]{1,0:T(8,128)(2,1)S(1)}, bf16[256,1408]{1,0:T(8,128)(2,1)S(1)}, u32[]{:S(2)}, u32[]{:S(2)}) collective-permute-start(bf16[256,1408]{1,0:T(8,128)(2,1)S(1)} %copy-done.9), channel_id=1, source_target_pairs={{4,8},{8,4},{5,9},{9,5},{6,10},{10,6},{7,11},{11,7},{20,24},{24,20... | collective-permute-start | bytes 2162696 | tf_op jit(solution)/shard_map/ppermute | solution.py:87
  122.9 30.8 %collective-permute-start.40 = (bf16[1408,256]{1,0:T(8,128)(2,1)S(1)}, bf16[1408,256]{1,0:T(8,128)(2,1)S(1)}, u32[]{:S(2)}, u32[]{:S(2)}) collective-permute-start(bf16[1408,256]{1,0:T(8,128)(2,1)S(1)} %copy-done.8), channel_id=1, source_target_pairs={{4,8},{8,4},{5,9},{9,5},{6,10},{10,6},{7,11},{11,7},{20,24},{24,20... | collective-permute-start | bytes 2162696 | tf_op jit(solution)/shard_map/ppermute | solution.py:87
  123.6 27.4 %collective-permute-start.25 = (bf16[256,1408]{1,0:T(8,128)(2,1)S(1)}, bf16[256,1408]{1,0:T(8,128)(2,1)S(1)}, u32[]{:S(2)}, u32[]{:S(2)}) collective-permute-start(bf16[256,1408]{1,0:T(8,128)(2,1)S(1)} %collective-permute-done.24), channel_id=1, source_target_pairs={{4,0},{8,12},{5,1},{9,13},{6,2},{10,14},{7,3},{11,15},{20,16},{24,... | collective-permute-start | bytes 2162696 | tf_op jit(solution)/shard_map/ppermute | solution.py:87
  136.3 52.6 %collective-permute-start.1 = (bf16[2,512,512]{2,1,0:T(8,128)(2,1)S(1)}, bf16[2,512,512]{2,1,0:T(8,128)(2,1)S(1)}, u32[]{:S(2)}, u32[]{:S(2)}) collective-permute-start(bf16[2,512,512]{2,1,0:T(8,128)(2,1)S(1)} %pad_maximum_fusion), channel_id=1, source_target_pairs={{0,1},{1,0},{2,3},{3,2},{4,5},{5,4},{6,7},{7,6},{8,9},{9,8},{10,11... | collective-permute-start | bytes 3145736 | tf_op jit(solution)/shard_map/ppermute | solution.py:87
  150.4 38.1 %collective-permute-start.7 = (bf16[256,1024]{1,0:T(8,128)(2,1)}, bf16[256,1024]{1,0:T(8,128)(2,1)S(1)}, u32[]{:S(2)}, u32[]{:S(2)}) collective-permute-start(bf16[256,1024]{1,0:T(8,128)(2,1)} %collective-permute-done.2), channel_id=1, source_target_pairs={{4,8},{8,4},{5,9},{9,5},{6,10},{10,6},{7,11},{11,7},{20,24},{24,20... | collective-permute-start | bytes 1572872 | tf_op jit(solution)/shard_map/ppermute | solution.py:87
  153.7 52.8 %collective-permute-start.27 = (bf16[256,1408]{1,0:T(8,128)(2,1)S(1)}, bf16[256,1408]{1,0:T(8,128)(2,1)}, u32[]{:S(2)}, u32[]{:S(2)}) collective-permute-start(bf16[256,1408]{1,0:T(8,128)(2,1)S(1)} %collective-permute-done.22), channel_id=1, source_target_pairs={{4,8},{8,4},{5,9},{9,5},{6,10},{10,6},{7,11},{11,7},{20,24},{24,20... | collective-permute-start | bytes 2162696 | tf_op jit(solution)/shard_map/ppermute | solution.py:87
  174.1 75.5 %collective-permute-start.35 = (bf16[256,1408]{1,0:T(8,128)(2,1)}, bf16[256,1408]{1,0:T(8,128)(2,1)}, u32[]{:S(2)}, u32[]{:S(2)}) collective-permute-start(bf16[256,1408]{1,0:T(8,128)(2,1)} %collective-permute-done.30), channel_id=1, source_target_pairs={{4,8},{8,4},{5,9},{9,5},{6,10},{10,6},{7,11},{11,7},{20,24},{24,20... | collective-permute-start | bytes 2162696 | tf_op jit(solution)/shard_map/ppermute | solution.py:87
  185.5 64.5 %collective-permute-start.43 = (bf16[1408,256]{1,0:T(8,128)(2,1)}, bf16[1408,256]{1,0:T(8,128)(2,1)}, u32[]{:S(2)}, u32[]{:S(2)}) collective-permute-start(bf16[1408,256]{1,0:T(8,128)(2,1)} %collective-permute-done.38), channel_id=1, source_target_pairs={{4,8},{8,4},{5,9},{9,5},{6,10},{10,6},{7,11},{11,7},{20,24},{24,20... | collective-permute-start | bytes 2162696 | tf_op jit(solution)/shard_map/ppermute | solution.py:87
  200.3 46.0 %collective-permute-start.26 = (bf16[256,1408]{1,0:T(8,128)(2,1)}, bf16[256,1408]{1,0:T(8,128)(2,1)}, u32[]{:S(2)}, u32[]{:S(2)}) collective-permute-start(bf16[256,1408]{1,0:T(8,128)(2,1)} %get-tuple-element.12), channel_id=1, source_target_pairs={{16,0},{0,16},{17,1},{1,17},{18,2},{2,18},{19,3},{3,19},{20,4},{4,... | collective-permute-start | bytes 2162696 | tf_op jit(solution)/shard_map/ppermute | solution.py:87
  200.9 29.8 %collective-permute-start.9 = (bf16[256,1024]{1,0:T(8,128)(2,1)S(1)}, bf16[256,1024]{1,0:T(8,128)(2,1)S(1)}, u32[]{:S(2)}, u32[]{:S(2)}) collective-permute-start(bf16[256,1024]{1,0:T(8,128)(2,1)S(1)} %get-tuple-element.28), channel_id=1, source_target_pairs={{16,0},{0,16},{17,1},{1,17},{18,2},{2,18},{19,3},{3,19},{20,4},{4,... | collective-permute-start | bytes 1572872 | tf_op jit(solution)/shard_map/ppermute | solution.py:87
  206.5 47.7 %collective-permute-start.34 = (bf16[256,1408]{1,0:T(8,128)(2,1)}, bf16[256,1408]{1,0:T(8,128)(2,1)S(1)}, u32[]{:S(2)}, u32[]{:S(2)}) collective-permute-start(bf16[256,1408]{1,0:T(8,128)(2,1)} %get-tuple-element.16), channel_id=1, source_target_pairs={{16,0},{0,16},{17,1},{1,17},{18,2},{2,18},{19,3},{3,19},{20,4},{4,... | collective-permute-start | bytes 2162696 | tf_op jit(solution)/shard_map/ppermute | solution.py:87
  251.3 32.8 %collective-permute-start.44 = (bf16[1408,256]{1,0:T(8,128)(2,1)}, bf16[1408,256]{1,0:T(8,128)(2,1)S(1)}, u32[]{:S(2)}, u32[]{:S(2)}) collective-permute-start(bf16[1408,256]{1,0:T(8,128)(2,1)} %collective-permute-done.43), channel_id=1, source_target_pairs={{4,0},{8,12},{5,1},{9,13},{6,2},{10,14},{7,3},{11,15},{20,16},{24,... | collective-permute-start | bytes 2162696 | tf_op jit(solution)/shard_map/ppermute | solution.py:87
  254.2 33.9 %collective-permute-start.29 = (bf16[256,1408]{1,0:T(8,128)(2,1)S(1)}, bf16[256,1408]{1,0:T(8,128)(2,1)S(1)}, u32[]{:S(2)}, u32[]{:S(2)}) collective-permute-start(bf16[256,1408]{1,0:T(8,128)(2,1)S(1)} %get-tuple-element.10), channel_id=1, source_target_pairs={{16,0},{0,16},{17,1},{1,17},{18,2},{2,18},{19,3},{3,19},{20,4},{4,... | collective-permute-start | bytes 2162696 | tf_op jit(solution)/shard_map/ppermute | solution.py:87
  (46 other events, 588.6 us)
